TPU v7x, 32 devices: a whole 2x2x4 slice. The times are simulated.
32 devices in a mesh: grp: 2 (over y), sp: 4 (over z), tp: 4 (over x, core).
Axes of the slice: x: 2, y: 2, z: 4, core: 2. Of those that a mesh axis runs over, the one named last changes fastest.
Arguments:
- starting_stream: bfloat16 [3072, 2048], P(('grp', 'sp'), 'tp'), parts along dimension 0, may hold values from -45 to 45
- multiplier_matrix: bfloat16 [2, 2048, 2048], P(None, 'sp', 'tp'), may hold values from -0.125 to 0.125
- memory_path_matrix: bfloat16 [2, 2048, 2048], P(None, 'sp', 'tp'), may hold values from -0.125 to 0.125
- filter_coefficients: bfloat16 [2, 4, 2048], P(None, None, 'tp'), may hold values from -3 to 3
- memory_valve_matrix: bfloat16 [2, 8, 256, 256], P(None, 'tp'), may hold values from -0.375 to 0.375
- entry_valve_matrix: bfloat16 [2, 8, 256, 256], P(None, 'tp'), may hold values from -0.375 to 0.375
- forgetting_parameters: float32 [2, 2048], P(None, 'tp'), may hold values from 3 to 15
- timestep_forgetting_multiplier: float32 [3072], P(('grp', 'sp')), parts along dimension 0, may hold values from 0.5 to 2
- spike_extra: float32 [3072, 2048], P(('grp', 'sp'), 'tp'), parts along dimension 0, may hold values from -0.7 to 0
- exit_projector_matrix: bfloat16 [2, 2048, 2048], P(None, 'tp', 'sp'), may hold values from -0.125 to 0.125
- prelude_rms_gains: float32 [2, 2048], replicated, may hold values from 0.1 to 1.9
- finishing_rms_gains: float32 [2048], P('tp'), may hold values from 0.1 to 1.9
Outputs:
- result: bfloat16 [3072, 2048], P(('grp', 'sp'), 'tp'), parts along dimension 0
There are 2 independent parts, one for each index of `grp`. A program takes and returns all parts, laid end to end along the dimension named above; an argument that names none is the same for every part. Nothing has to cross between parts.
All inputs are finite; a program needn't handle non-finite values.
Results may differ from a plain program's by a relative error of at most 0.015.
Values may be sent and summed in bfloat16 or wider, within the bound.
No kernel may reach another device: no remote copies, remote signals or barrier semaphores. Data moves between devices by JAX's collectives and lax.ppermute only.
A program may use at most 64 MiB of HBM per device.

v0:
```python
import functools

import jax
import jax.numpy as jnp
from jax import lax
from jax.experimental import pallas as pl
from jax.experimental.pallas import tpu as pltpu
from jax.sharding import PartitionSpec as P


EPSILON = 1e-06
SQUASH_POWER = 8.0
LANES = 128
SUBLANES = 8
HALO = 16
F32 = jnp.float32
BF16 = jnp.bfloat16

HBM = pl.BlockSpec(memory_space=pltpu.MemorySpace.HBM)
VMEM = pl.BlockSpec(memory_space=pltpu.MemorySpace.VMEM)


def swap(value, axis, mask):
    count = lax.axis_size(axis)
    return lax.ppermute(value, axis, [(i, i ^ mask) for i in range(count)])


def shift(value, axis, steps):
    count = lax.axis_size(axis)
    return lax.ppermute(value, axis, [(i, i + steps) for i in range(count - steps)])


def spread(matrices, layer, by_sp):
    groups = lax.axis_size("grp")
    count = lax.axis_size("sp")
    size, cols = matrices[0].shape[1] // groups, matrices[0].shape[2]
    first = lax.axis_index("grp") * size
    own = [lax.dynamic_slice(w, (layer, first, 0), (1, size, cols)) for w in matrices]
    mine = jnp.concatenate(own, axis=0)
    held, source = {0: mine}, {}
    bit = count // 2
    while bit:
        for offset, value in sorted(held.items()):
            held[offset | bit] = swap(value, "sp", bit)
            source[offset | bit] = (offset, bit)
        bit //= 2
    parts, others = [], {}
    for k in range(1, count):
        parts.append(held[k])
        for q in range(1, groups):
            offset, bit = source[k]
            if by_sp and offset:
                others[k, q] = swap(others[offset, q], "sp", bit)
            else:
                others[k, q] = swap(held[k], "grp", q)
            parts.append(others[k, q])
    return parts


def gather_tp(own):
    held = {0: own}
    bit = lax.axis_size("tp") // 2
    while bit:
        for offset, value in list(held.items()):
            held[offset | bit] = swap(value, "tp", bit)
        bit //= 2
    return [held[k] for k in range(len(held))]


def start_parts(layer, place, whole, parts, scratch, sems, by_columns):
    if not parts:
        copies = [pltpu.make_async_copy(whole, scratch, sems.at[0])]
        copies[0].start()
        return copies
    groups, count = lax.axis_size("grp"), lax.axis_size("sp")
    g, s = lax.axis_index("grp"), lax.axis_index("sp")
    _, rows, cols = whole.shape
    step = rows // groups
    plan = [(whole.at[layer], s, 0, rows)]
    k = 0
    for d in range(1, count):
        for q in range(groups):
            plan.append((parts[k].at[place], s ^ d, (g ^ q) * step, step))
            k += 1
    copies = []
    for i, (src, block, first, size) in enumerate(plan):
        if by_columns:
            dst = scratch.at[
                pl.ds(pl.multiple_of(first, step), size),
                pl.ds(pl.multiple_of(block * cols, LANES), cols),
            ]
        else:
            dst = scratch.at[pl.ds(pl.multiple_of(block * rows + first, step), size), :]
        copies.append(pltpu.make_async_copy(src, dst, sems.at[i]))
    for c in copies:
        c.start()
    return copies


def recur_kernel(layer, place, m, nw, *refs):
    xs, gain, ws = refs[:m], refs[m], refs[m + 1 : m + 1 + nw]
    normed, out, x_s, w_s, x_sem, w_sem = refs[m + 1 + nw :]
    t = lax.axis_index("tp")
    rows, width = x_s.shape
    c = width // m
    xc = []
    for j in range(m):
        dst = x_s.at[:, pl.ds(pl.multiple_of((t ^ j) * c, LANES), c)]
        xc.append(pltpu.make_async_copy(xs[j], dst, x_sem.at[j]))
    for copy in xc:
        copy.start()
    wc = start_parts(layer, place, ws[0], ws[1:], w_s, w_sem, False)
    for copy in xc:
        copy.wait()
    chunk = 2 * SUBLANES

    def one(i, _):
        at = pl.ds(pl.multiple_of(i * chunk, chunk), chunk)
        x = x_s[at, :].astype(F32)
        mean = jnp.sum(x * x, axis=1, keepdims=True) * (1.0 / width)
        normed[at, :] = (x * lax.rsqrt(mean + EPSILON) * gain[...]).astype(BF16)
        return 0

    lax.fori_loop(0, rows // chunk, one, 0, unroll=5 if rows // chunk % 5 == 0 else 4)
    for copy in wc:
        copy.wait()
    out[...] = jnp.dot(normed[...], w_s[...], preferred_element_type=F32).astype(BF16)


def branch_kernel(layer, place, pre, nw, *refs):
    normed, ws = refs[0], refs[1 : 1 + nw]
    out, w_s, w_sem = refs[1 + nw :]
    for copy in start_parts(layer, place, ws[0], ws[1:], w_s, w_sem, False):
        copy.wait()
    branch = jnp.dot(normed[pre:, :], w_s[...], preferred_element_type=F32)
    out[...] = jax.nn.gelu(branch.astype(BF16).astype(F32))


def one_minus_exp(y):
    series = y * (1.0 / 8.0) + 1.0
    for n in (7.0, 6.0, 5.0, 4.0, 3.0, 2.0):
        series = series * (y * (1.0 / n)) + 1.0
    return jnp.where(y > -0.3, -y * series, 1.0 - jnp.exp(y))


def scan_kernel(pre, *refs):
    rec, refs = refs[0], refs[1:]
    if pre == 0:
        halo, refs = refs[0], refs[1:]
    taps, valve_r, valve_i, rate, tmul, spike = refs[:6]
    acum, hcum, seg, tot, ext, conv, gate_r, gate_i, spike_s, sem = refs[6:]
    rows, channels = spike.shape
    fetch = pltpu.make_async_copy(spike, spike_s, sem.at[0])
    fetch.start()
    blocks = valve_r.shape[0]
    bw = channels // blocks
    ntap = taps.shape[0]
    if pre == 0:
        ext[:HALO, :] = halo[...].astype(F32)
    ext[HALO - pre :, :] = rec[...].astype(F32)
    chunk = 4 * SUBLANES
    for first in range(0, rows, chunk):
        acc = None
        for k in range(ntap):
            lo = HALO + first - (ntap - 1) + k
            term = ext[lo : lo + chunk, :] * taps[k : k + 1, :].astype(F32)
            acc = term if acc is None else acc + term
        conv[first : first + chunk, :] = acc.astype(BF16)
    for b in range(blocks):
        cols = slice(b * bw, (b + 1) * bw)
        gate_r[:, cols] = jnp.dot(conv[:, cols], valve_r[b], preferred_element_type=F32)
        gate_i[:, cols] = jnp.dot(conv[:, cols], valve_i[b], preferred_element_type=F32)
    step = 2 * SUBLANES
    fetch.wait()

    def one(i, _):
        at = pl.ds(pl.multiple_of(i * step, step), step)
        reset = 0.5 * jnp.tanh(0.5 * gate_r[at, :]) + 0.5
        inject = 0.5 * jnp.tanh(0.5 * gate_i[at, :]) + 0.5
        logk = reset * rate[...] * tmul[at, :] + spike_s[at, :]
        keep = jnp.exp(logk)
        driven = inject * conv[at, :].astype(F32) * jnp.sqrt(one_minus_exp(2.0 * logk))
        for b in range(channels // LANES):
            lanes = slice(b * LANES, (b + 1) * LANES)
            acum[b, at, :] = keep[:, lanes]
            hcum[b, at, :] = driven[:, lanes]
        return 0

    lax.fori_loop(0, rows // step, one, 0, unroll=2)
    length = rows // SUBLANES

    def scan(i, carry):
        a_all, h_all = carry
        at = pl.ds(i, SUBLANES, stride=length)
        nxt_a, nxt_h = [], []
        for b in range(channels // LANES):
            a = acum[b, at, :]
            h = a * h_all[b] + hcum[b, at, :]
            aa = a * a_all[b]
            acum[b, at, :] = aa
            hcum[b, at, :] = h
            nxt_a.append(aa)
            nxt_h.append(h)
        return tuple(nxt_a), tuple(nxt_h)

    nl = channels // LANES
    ones = tuple(jnp.ones((SUBLANES, LANES), F32) for _ in range(nl))
    zeros = tuple(jnp.zeros((SUBLANES, LANES), F32) for _ in range(nl))
    a_all, h_all = lax.fori_loop(0, length, scan, (ones, zeros), unroll=4)
    for b in range(nl):
        lanes = slice(b * LANES, (b + 1) * LANES)
        ca, ch = jnp.ones((1, LANES), F32), jnp.zeros((1, LANES), F32)
        for i in range(SUBLANES):
            seg[i : i + 1, lanes] = ch
            seg[SUBLANES + i : SUBLANES + i + 1, lanes] = ca
            ch = a_all[b][i : i + 1, :] * ch + h_all[b][i : i + 1, :]
            ca = ca * a_all[b][i : i + 1, :]
        tot[0:1, lanes] = ca
        tot[1:2, lanes] = ch


def exit_kernel(layer, place, m, nc, nw, *refs):
    gelu, acum, hcum, seg = refs[:4]
    before = refs[4 : 4 + nc]
    ws = refs[4 + nc : 4 + nc + nw]
    send, keep, mixed, w_s, w_sem = refs[4 + nc + nw :]
    copies = start_parts(layer, place, ws[0], ws[1:], w_s, w_sem, True)
    rows, channels = gelu.shape
    t = lax.axis_index("tp")
    carry = jnp.zeros((1, channels), F32)
    for part in before:
        carry = part[0:1, :] * carry + part[1:2, :]
    entry = seg[0:SUBLANES, :] + seg[SUBLANES : 2 * SUBLANES, :] * carry
    length = rows // SUBLANES
    for i in range(SUBLANES):
        at = slice(i * length, (i + 1) * length)
        for b in range(channels // LANES):
            lanes = slice(b * LANES, (b + 1) * LANES)
            state = hcum[b, at, :] + acum[b, at, :] * entry[i : i + 1, lanes]
            mixed[at, lanes] = (gelu[at, lanes] * state).astype(BF16)
    for copy in copies:
        copy.wait()
    c = w_s.shape[1] // m
    for j in [k for k in range(m) if k & 1] + [k for k in range(m) if not k & 1]:
        w = w_s[:, pl.ds(pl.multiple_of((t ^ j) * c, LANES), c)]
        out = jnp.dot(mixed[...], w, preferred_element_type=F32).astype(BF16)
        (send if j & 1 else keep)[j >> 1] = out


def cost(flops, nbytes):
    return pl.CostEstimate(flops=int(flops), bytes_accessed=int(nbytes), transcendentals=0)


def on_device(
    starting_stream,
    multiplier_matrix,
    memory_path_matrix,
    filter_coefficients,
    memory_valve_matrix,
    entry_valve_matrix,
    forgetting_parameters,
    timestep_forgetting_multiplier,
    spike_extra,
    exit_projector_matrix,
    prelude_rms_gains,
    finishing_rms_gains,
):
    rows, own_width = starting_stream.shape
    layers, shard_rows, channels = memory_path_matrix.shape
    m = lax.axis_size("tp")
    n = lax.axis_size("sp")
    width = shard_rows * n
    shape = jax.ShapeDtypeStruct
    rates = -SQUASH_POWER * jax.nn.softplus(-forgetting_parameters)
    tmul = timestep_forgetting_multiplier[:, None]
    params = pltpu.CompilerParams(vmem_limit_bytes=16 * 1024 * 1024)

    chunks, places = {}, {}
    named = {"m": memory_path_matrix, "b": multiplier_matrix, "e": exit_projector_matrix}
    for layer in range(layers):
        groups = ["m", "b", "e"]
        if named["e"].shape[2] % LANES:
            shard = named["e"][layer]
            chunks[f"e{layer}"] = [lax.all_gather(shard, "sp", axis=1, tiled=True)]
            places[f"e{layer}"] = 0
            groups = ["m", "b"]
        for kinds in groups:
            matrices = [named[kind] for kind in kinds]
            parts = spread(matrices, layer, kinds == "e" and layer == layers - 1)
            for place, kind in enumerate(kinds):
                chunks[f"{kind}{layer}"] = [named[kind]] + parts
                places[f"{kind}{layer}"] = place

    own = starting_stream
    for layer in range(layers):
        pre = HALO if layer == 0 else 0
        lead = [shift(own[rows - HALO :], "sp", 1)] if pre else []
        pieces = gather_tp(jnp.concatenate(lead + [own], axis=0))
        ws = chunks[f"m{layer}"]
        normed, recurrent = pl.pallas_call(
            functools.partial(recur_kernel, layer, places[f"m{layer}"], m, len(ws)),
            out_shape=(
                shape((pre + rows, width), BF16),
                shape((pre + rows, channels), BF16),
            ),
            in_specs=[HBM] * m + [VMEM] + [HBM] * len(ws),
            out_specs=(VMEM, VMEM),
            scratch_shapes=[
                pltpu.VMEM((pre + rows, width), BF16),
                pltpu.VMEM((width, channels), BF16),
                pltpu.SemaphoreType.DMA((m,)),
                pltpu.SemaphoreType.DMA((len(ws),)),
            ],
            compiler_params=params,
            cost_estimate=cost(4 * rows * width * channels, 8 * rows * width),
            name="recur",
        )(*pieces, prelude_rms_gains[layer : layer + 1], *ws)
        halo = []
        if not pre:
            halo = [shift(recurrent[rows - HALO :], "sp", 1)]
        ws = chunks[f"b{layer}"]
        gelu = pl.pallas_call(
            functools.partial(branch_kernel, layer, places[f"b{layer}"], pre, len(ws)),
            out_shape=shape((rows, channels), F32),
            in_specs=[VMEM] + [HBM] * len(ws),
            out_specs=VMEM,
            scratch_shapes=[
                pltpu.VMEM((width, channels), BF16),
                pltpu.SemaphoreType.DMA((len(ws),)),
            ],
            compiler_params=params,
            cost_estimate=cost(4 * rows * width * channels, 8 * rows * width),
            name="branch",
        )(normed, *ws)
        acum, hcum, seg, tot = pl.pallas_call(
            functools.partial(scan_kernel, pre),
            out_shape=(
                shape((channels // LANES, rows, LANES), F32),
                shape((channels // LANES, rows, LANES), F32),
                shape((2 * SUBLANES, channels), F32),
                shape((2, channels), F32),
            ),
            in_specs=[VMEM] * (6 + len(halo)) + [HBM],
            out_specs=(VMEM,) * 4,
            scratch_shapes=[
                pltpu.VMEM((HALO + rows, channels), F32),
                pltpu.VMEM((rows, channels), BF16),
                pltpu.VMEM((rows, channels), F32),
                pltpu.VMEM((rows, channels), F32),
                pltpu.VMEM((rows, channels), F32),
                pltpu.SemaphoreType.DMA((1,)),
            ],
            compiler_params=params,
            cost_estimate=cost(8 * rows * width * channels, 8 * rows * width),
            name="scan",
        )(
            recurrent,
            *halo,
            filter_coefficients[layer],
            memory_valve_matrix[layer],
            entry_valve_matrix[layer],
            rates[layer : layer + 1],
            tmul,
            spike_extra,
        )
        before = [shift(tot, "sp", k) for k in range(n - 1, 0, -1)]
        ws = chunks[f"e{layer}"]
        send, keep = pl.pallas_call(
            functools.partial(exit_kernel, layer, places[f"e{layer}"], m, len(before), len(ws)),
            out_shape=(
                shape((m // 2, rows, own_width), BF16),
                shape((m - m // 2, rows, own_width), BF16),
            ),
            in_specs=[VMEM] * (4 + len(before)) + [HBM] * len(ws),
            out_specs=(VMEM, VMEM),
            scratch_shapes=[
                pltpu.VMEM((rows, channels), BF16),
                pltpu.VMEM((channels, width), BF16),
                pltpu.SemaphoreType.DMA((len(ws),)),
            ],
            compiler_params=params,
            cost_estimate=cost(4 * rows * width * channels, 8 * rows * width),
            name="exit",
        )(gelu, acum, hcum, seg, *before, *ws)
        bit = 1
        while True:
            arrived = swap(send, "tp", bit)
            total = keep.astype(F32) + arrived.astype(F32)
            bit *= 2
            if bit == m:
                break
            send, keep = total[1::2].astype(BF16), total[0::2]
        own = (own.astype(F32) + total[0]).astype(BF16)
    floats = own.astype(F32)
    squares = jnp.sum(floats * floats, axis=1)
    squares = sum([swap(squares, "tp", k) for k in range(1, m)], squares)
    inv_rms = lax.rsqrt(squares / width + EPSILON)
    return (floats * inv_rms[:, None] * finishing_rms_gains[None, :]).astype(BF16)


def solution(mesh):
    def step(*args):
        run = jax.shard_map(
            on_device,
            mesh=mesh,
            in_specs=(
                P(("grp", "sp"), "tp"),
                P(None, "sp", "tp"),
                P(None, "sp", "tp"),
                P(None, None, "tp"),
                P(None, "tp", None, None),
                P(None, "tp", None, None),
                P(None, "tp"),
                P(("grp", "sp")),
                P(("grp", "sp"), "tp"),
                P(None, "tp", "sp"),
                P(),
                P("tp"),
            ),
            out_specs=P(("grp", "sp"), "tp"),
            check_vma=False,
        )
        jax.eval_shape(run, *args)
        return run(*args)

    return step
```

profile of v0, /device:TPU:0, one launch (start us, length us, event | category | flops | bytes accessed | tf_op | source)
XLA Modules:
  0.0 202.6 jit_solution(1205287271453575599)
XLA Ops:
  1.2 4.1 %collective-permute-start.6 = (bf16[1,256,512]{2,1,0:T(8,128)(2,1)S(1)}, bf16[1,256,512]{2,1,0:T(8,128)(2,1)S(1)}, u32[]{:S(2)}, u32[]{:S(2)}) collective-permute-start(bf16[1,256,512]{2,1,0:T(8,128)(2,1)S(1)} %get-tuple-element.44), channel_id=1, source_target_pairs={{0,8},{4,12},{8,0},{12,4},{1,9},{5,13},{9,1},{13,5},{2,10},{6,14},... | collective-permute-start | bytes 786440 | tf_op jit(solution)/shard_map/ppermute | solution.py:25
  11.3 2.9 %collective-permute-start.21 = (bf16[1,256,512]{2,1,0:T(8,128)(2,1)S(1)}, bf16[1,256,512]{2,1,0:T(8,128)(2,1)S(1)}, u32[]{:S(2)}, u32[]{:S(2)}) collective-permute-start(bf16[1,256,512]{2,1,0:T(8,128)(2,1)S(1)} %get-tuple-element.40), channel_id=1, source_target_pairs={{0,8},{4,12},{8,0},{12,4},{1,9},{5,13},{9,1},{13,5},{2,10},{6,14},... | collective-permute-start | bytes 786440 | tf_op jit(solution)/shard_map/ppermute | solution.py:25
  14.2 3.9 %collective-permute-done = bf16[16,512]{1,0:T(8,128)(2,1)S(1)} collective-permute-done((bf16[16,512]{1,0:T(8,128)(2,1)S(1)}, bf16[16,512]{1,0:T(8,128)(2,1)S(1)}, u32[]{:S(2)}, u32[]{:S(2)}) %collective-permute-start) | collective-permute-done | bytes 16416 | tf_op jit(solution)/shard_map/ppermute | solution.py:30
  22.4 5.0 %collective-permute-done.2.refs_2_ = bf16[400,512]{1,0:T(8,128)(2,1)S(1)} collective-permute-done((bf16[400,512]{1,0:T(8,128)(2,1)S(1)}, bf16[400,512]{1,0:T(8,128)(2,1)S(1)}, u32[]{:S(2)}, u32[]{:S(2)}) %collective-permute-start.2) | collective-permute-done | bytes 409632 | tf_op jit(solution)/shard_map/ppermute | solution.py:25
  27.4 7.6 %collective-permute-done.12.refs_4_ = bf16[1,256,512]{2,1,0:T(8,128)(2,1)S(1)} collective-permute-done((bf16[1,256,512]{2,1,0:T(8,128)(2,1)S(1)}, bf16[1,256,512]{2,1,0:T(8,128)(2,1)S(1)}, u32[]{:S(2)}, u32[]{:S(2)}) %collective-permute-start.12) | collective-permute-done | bytes 262176 | tf_op jit(solution)/shard_map/ppermute | solution.py:25
  36.9 2.9 %collective-permute-done.21.refs_10_ = bf16[1,256,512]{2,1,0:T(8,128)(2,1)S(1)} collective-permute-done((bf16[1,256,512]{2,1,0:T(8,128)(2,1)S(1)}, bf16[1,256,512]{2,1,0:T(8,128)(2,1)S(1)}, u32[]{:S(2)}, u32[]{:S(2)}) %collective-permute-start.21) | collective-permute-done | bytes 262176 | tf_op jit(solution)/shard_map/ppermute | solution.py:25
  44.0 5.0 %collective-permute-done.5.refs_7_ = bf16[1,256,512]{2,1,0:T(8,128)(2,1)S(1)} collective-permute-done((bf16[1,256,512]{2,1,0:T(8,128)(2,1)S(1)}, bf16[1,256,512]{2,1,0:T(8,128)(2,1)S(1)}, u32[]{:S(2)}, u32[]{:S(2)}) %collective-permute-start.5) | collective-permute-done | bytes 262176 | tf_op jit(solution)/shard_map/ppermute | solution.py:25
  50.0 2.9 %collective-permute-done.9.refs_11_ = bf16[1,256,512]{2,1,0:T(8,128)(2,1)S(1)} collective-permute-done((bf16[1,256,512]{2,1,0:T(8,128)(2,1)S(1)}, bf16[1,256,512]{2,1,0:T(8,128)(2,1)S(1)}, u32[]{:S(2)}, u32[]{:S(2)}) %collective-permute-start.9) | collective-permute-done | bytes 262176 | tf_op jit(solution)/shard_map/ppermute | solution.py:25
  67.3 4.0 %scan.2 = (f32[4,384,128]{2,1,0:T(8,128)S(1)}, f32[4,384,128]{2,1,0:T(8,128)S(1)}, f32[16,512]{1,0:T(8,128)S(1)}, f32[2,512]{1,0:T(2,128)S(1)}) custom-call(bf16[400,512]{1,0:T(8,128)(2,1)S(1)} %get-tuple-element.22.refs_0_, bf16[4,512]{1,0:T(4,128)(2,1)S(1)} %get-tuple-element.52.refs_1_, bf16[2,256,256]{2,1,0:T(8,128)(2,1)S(1)} %get-tuple-element.55.refs_2_, ...), custom_call_target="tpu_custom_call" | custom-call | flops 3221225472 | bytes 6291456 | tf_op jit(solution)/shard_map/scan/pallas_call | solution.py:335
  73.5 6.3 %collective-permute-start.16 = (f32[2,512]{1,0:T(2,128)S(1)}, f32[2,512]{1,0:T(2,128)S(1)}, u32[]{:S(2)}, u32[]{:S(2)}) collective-permute-start(f32[2,512]{1,0:T(2,128)S(1)} %get-tuple-element.26), channel_id=1, source_target_pairs={{0,12},{1,13},{2,14},{3,15},{16,28},{17,29},{18,30},{19,31}} | collective-permute-start | bytes 12296 | tf_op jit(solution)/shard_map/ppermute | solution.py:30
  81.1 3.7 %collective-permute-done.15.refs_7_ = bf16[1,256,512]{2,1,0:T(8,128)(2,1)S(1)} collective-permute-done((bf16[1,256,512]{2,1,0:T(8,128)(2,1)S(1)}, bf16[1,256,512]{2,1,0:T(8,128)(2,1)S(1)}, u32[]{:S(2)}, u32[]{:S(2)}) %collective-permute-start.15) | collective-permute-done | bytes 262176 | tf_op jit(solution)/shard_map/ppermute | solution.py:25
  84.8 3.5 %collective-permute-start.18 = (f32[2,512]{1,0:T(2,128)S(1)}, f32[2,512]{1,0:T(2,128)S(1)}, u32[]{:S(2)}, u32[]{:S(2)}) collective-permute-start(f32[2,512]{1,0:T(2,128)S(1)} %get-tuple-element.26), channel_id=1, source_target_pairs={{0,4},{4,8},{8,12},{1,5},{5,9},{9,13},{2,6},{6,10},{10,14},{3,7},{... | collective-permute-start | bytes 12296 | tf_op jit(solution)/shard_map/ppermute | solution.py:30
  95.4 3.9 %collective-permute-start.32 = (bf16[1,256,512]{2,1,0:T(8,128)(2,1)S(1)}, bf16[1,256,512]{2,1,0:T(8,128)(2,1)S(1)}, u32[]{:S(2)}, u32[]{:S(2)}) collective-permute-start(bf16[1,256,512]{2,1,0:T(8,128)(2,1)S(1)} %get-tuple-element.43), channel_id=1, source_target_pairs={{0,8},{4,12},{8,0},{12,4},{1,9},{5,13},{9,1},{13,5},{2,10},{6,14},... | collective-permute-start | bytes 786440 | tf_op jit(solution)/shard_map/ppermute | solution.py:25
  99.3 5.8 %collective-permute-done.26 = bf16[1,384,512]{2,1,0:T(8,128)(2,1)S(1)} collective-permute-done((bf16[1,384,512]{2,1,0:T(8,128)(2,1)S(1)}, bf16[1,384,512]{2,1,0:T(8,128)(2,1)S(1)}, u32[]{:S(2)}, u32[]{:S(2)}) %collective-permute-start.26) | collective-permute-done | bytes 393248 | tf_op jit(solution)/shard_map/ppermute | solution.py:25
  109.1 3.1 %collective-permute-start.38 = (bf16[1,256,512]{2,1,0:T(8,128)(2,1)S(1)}, bf16[1,256,512]{2,1,0:T(8,128)(2,1)S(1)}, u32[]{:S(2)}, u32[]{:S(2)}) collective-permute-start(bf16[1,256,512]{2,1,0:T(8,128)(2,1)S(1)} %get-tuple-element.41), channel_id=1, source_target_pairs={{0,8},{4,12},{8,0},{12,4},{1,9},{5,13},{9,1},{13,5},{2,10},{6,14},... | collective-permute-start | bytes 786440 | tf_op jit(solution)/shard_map/ppermute | solution.py:25
  112.7 9.8 %collective-permute-done.30.refs_6_ = bf16[1,256,512]{2,1,0:T(8,128)(2,1)S(1)} collective-permute-done((bf16[1,256,512]{2,1,0:T(8,128)(2,1)S(1)}, bf16[1,256,512]{2,1,0:T(8,128)(2,1)S(1)}, u32[]{:S(2)}, u32[]{:S(2)}) %collective-permute-start.30) | collective-permute-done | bytes 262176 | tf_op jit(solution)/shard_map/ppermute | solution.py:25
  123.0 7.6 %collective-permute-done.38.refs_4_ = bf16[1,256,512]{2,1,0:T(8,128)(2,1)S(1)} collective-permute-done((bf16[1,256,512]{2,1,0:T(8,128)(2,1)S(1)}, bf16[1,256,512]{2,1,0:T(8,128)(2,1)S(1)}, u32[]{:S(2)}, u32[]{:S(2)}) %collective-permute-start.38) | collective-permute-done | bytes 262176 | tf_op jit(solution)/shard_map/ppermute | solution.py:25
  138.9 5.6 %collective-permute-done.31.refs_7_ = bf16[1,256,512]{2,1,0:T(8,128)(2,1)S(1)} collective-permute-done((bf16[1,256,512]{2,1,0:T(8,128)(2,1)S(1)}, bf16[1,256,512]{2,1,0:T(8,128)(2,1)S(1)}, u32[]{:S(2)}, u32[]{:S(2)}) %collective-permute-start.31) | collective-permute-done | bytes 262176 | tf_op jit(solution)/shard_map/ppermute | solution.py:25
  144.5 3.7 %collective-permute-done.35.refs_11_ = bf16[1,256,512]{2,1,0:T(8,128)(2,1)S(1)} collective-permute-done((bf16[1,256,512]{2,1,0:T(8,128)(2,1)S(1)}, bf16[1,256,512]{2,1,0:T(8,128)(2,1)S(1)}, u32[]{:S(2)}, u32[]{:S(2)}) %collective-permute-start.35) | collective-permute-done | bytes 262176 | tf_op jit(solution)/shard_map/ppermute | solution.py:25
  152.6 3.9 %collective-permute-start.42 = (bf16[16,512]{1,0:T(8,128)(2,1)S(1)}, bf16[16,512]{1,0:T(8,128)(2,1)S(1)}, u32[]{:S(2)}, u32[]{:S(2)}) collective-permute-start(bf16[16,512]{1,0:T(8,128)(2,1)S(1)} %slice.63), channel_id=1, source_target_pairs={{0,4},{4,8},{8,12},{1,5},{5,9},{9,13},{2,6},{6,10},{10,14},{3,7},{... | collective-permute-start | bytes 49160 | tf_op jit(solution)/shard_map/ppermute | solution.py:30
  166.6 4.1 %scan.3 = (f32[4,384,128]{2,1,0:T(8,128)S(1)}, f32[4,384,128]{2,1,0:T(8,128)S(1)}, f32[16,512]{1,0:T(8,128)S(1)}, f32[2,512]{1,0:T(2,128)S(1)}) custom-call(bf16[384,512]{1,0:T(8,128)(2,1)S(1)} %get-tuple-element.30.refs_0_, bf16[16,512]{1,0:T(8,128)(2,1)S(1)} %collective-permute-done.42.refs_1_, bf16[4,512]{1,0:T(4,128)(2,1)S(1)} %get-tuple-element.51.refs_2_, ...), custom_call_target="tpu_custom_call" | custom-call | flops 3221225472 | bytes 6291456 | tf_op jit(solution)/shard_map/scan/pallas_call | solution.py:335
  170.6 4.2 %collective-permute-start.43 = (f32[2,512]{1,0:T(2,128)S(1)}, f32[2,512]{1,0:T(2,128)S(1)}, u32[]{:S(2)}, u32[]{:S(2)}) collective-permute-start(f32[2,512]{1,0:T(2,128)S(1)} %get-tuple-element.34), channel_id=1, source_target_pairs={{0,12},{1,13},{2,14},{3,15},{16,28},{17,29},{18,30},{19,31}} | collective-permute-start | bytes 12296 | tf_op jit(solution)/shard_map/ppermute | solution.py:30
  177.3 3.6 %collective-permute-start.45 = (f32[2,512]{1,0:T(2,128)S(1)}, f32[2,512]{1,0:T(2,128)S(1)}, u32[]{:S(2)}, u32[]{:S(2)}) collective-permute-start(f32[2,512]{1,0:T(2,128)S(1)} %get-tuple-element.34), channel_id=1, source_target_pairs={{0,4},{4,8},{8,12},{1,5},{5,9},{9,13},{2,6},{6,10},{10,14},{3,7},{... | collective-permute-start | bytes 12296 | tf_op jit(solution)/shard_map/ppermute | solution.py:30
  187.1 10.6 %collective-permute-done.53 = bf16[1,384,512]{2,1,0:T(8,128)(2,1)S(1)} collective-permute-done((bf16[1,384,512]{2,1,0:T(8,128)(2,1)S(1)}, bf16[1,384,512]{2,1,0:T(8,128)(2,1)S(1)}, u32[]{:S(2)}, u32[]{:S(2)}) %collective-permute-start.53) | collective-permute-done | bytes 393248 | tf_op jit(solution)/shard_map/ppermute | solution.py:25
  (143 shorter events, 84.5 us)
Async XLA Ops:
  1.2 18.5 %collective-permute-start.6 = (bf16[1,256,512]{2,1,0:T(8,128)(2,1)S(1)}, bf16[1,256,512]{2,1,0:T(8,128)(2,1)S(1)}, u32[]{:S(2)}, u32[]{:S(2)}) collective-permute-start(bf16[1,256,512]{2,1,0:T(8,128)(2,1)S(1)} %get-tuple-element.44), channel_id=1, source_target_pairs={{0,8},{4,12},{8,0},{12,4},{1,9},{5,13},{9,1},{13,5},{2,10},{6,14},... | collective-permute-start | bytes 786440 | tf_op jit(solution)/shard_map/ppermute | solution.py:25
  5.4 16.9 %collective-permute-start.4 = (bf16[1,256,512]{2,1,0:T(8,128)(2,1)S(1)}, bf16[1,256,512]{2,1,0:T(8,128)(2,1)S(1)}, u32[]{:S(2)}, u32[]{:S(2)}) collective-permute-start(bf16[1,256,512]{2,1,0:T(8,128)(2,1)S(1)} %get-tuple-element.44), channel_id=1, source_target_pairs={{0,4},{4,0},{8,12},{12,8},{1,5},{5,1},{9,13},{13,9},{2,6},{6,2},{1... | collective-permute-start | bytes 786440 | tf_op jit(solution)/shard_map/ppermute | solution.py:25
  11.1 24.0 %collective-permute-start.12 = (bf16[1,256,512]{2,1,0:T(8,128)(2,1)S(1)}, bf16[1,256,512]{2,1,0:T(8,128)(2,1)S(1)}, u32[]{:S(2)}, u32[]{:S(2)}) collective-permute-start(bf16[1,256,512]{2,1,0:T(8,128)(2,1)S(1)} %get-tuple-element.42), channel_id=1, source_target_pairs={{0,8},{4,12},{8,0},{12,4},{1,9},{5,13},{9,1},{13,5},{2,10},{6,14},... | collective-permute-start | bytes 786440 | tf_op jit(solution)/shard_map/ppermute | solution.py:25
  11.3 28.5 %collective-permute-start.21 = (bf16[1,256,512]{2,1,0:T(8,128)(2,1)S(1)}, bf16[1,256,512]{2,1,0:T(8,128)(2,1)S(1)}, u32[]{:S(2)}, u32[]{:S(2)}) collective-permute-start(bf16[1,256,512]{2,1,0:T(8,128)(2,1)S(1)} %get-tuple-element.40), channel_id=1, source_target_pairs={{0,8},{4,12},{8,0},{12,4},{1,9},{5,13},{9,1},{13,5},{2,10},{6,14},... | collective-permute-start | bytes 786440 | tf_op jit(solution)/shard_map/ppermute | solution.py:25
  19.7 21.7 %collective-permute-start.8 = (bf16[1,256,512]{2,1,0:T(8,128)(2,1)S(1)}, bf16[1,256,512]{2,1,0:T(8,128)(2,1)S(1)}, u32[]{:S(2)}, u32[]{:S(2)}) collective-permute-start(bf16[1,256,512]{2,1,0:T(8,128)(2,1)S(1)} %collective-permute-done.6.refs_8_), channel_id=1, source_target_pairs={{0,4},{4,0},{8,12},{12,8},{1,5},{5,1},{9,13},{13,9},{2,6},{6,2},{1... | collective-permute-start | bytes 786440 | tf_op jit(solution)/shard_map/ppermute | solution.py:25
  22.3 19.7 %collective-permute-start.1 = (bf16[400,512]{1,0:T(8,128)(2,1)S(1)}, bf16[400,512]{1,0:T(8,128)(2,1)S(1)}, u32[]{:S(2)}, u32[]{:S(2)}) collective-permute-start(bf16[400,512]{1,0:T(8,128)(2,1)S(1)} %constant_dynamic-update-slice_fusion.refs_0_), channel_id=1, source_target_pairs={{0,1},{1,0},{2,3},{3,2},{4,5},{5,4},{6,7},{7,6},{8,9},{9,8},{10,11... | collective-permute-start | bytes 1228808 | tf_op jit(solution)/shard_map/ppermute | solution.py:25
  27.4 27.1 %collective-permute-start.3 = (bf16[400,512]{1,0:T(8,128)(2,1)S(1)}, bf16[400,512]{1,0:T(8,128)(2,1)S(1)}, u32[]{:S(2)}, u32[]{:S(2)}) collective-permute-start(bf16[400,512]{1,0:T(8,128)(2,1)S(1)} %collective-permute-done.2.refs_2_), channel_id=1, source_target_pairs={{0,1},{1,0},{2,3},{3,2},{4,5},{5,4},{6,7},{7,6},{8,9},{9,8},{10,11... | collective-permute-start | bytes 1228808 | tf_op jit(solution)/shard_map/ppermute | solution.py:25
  41.9 16.7 %collective-permute-start.10 = (bf16[1,256,512]{2,1,0:T(8,128)(2,1)S(1)}, bf16[1,256,512]{2,1,0:T(8,128)(2,1)S(1)}, u32[]{:S(2)}, u32[]{:S(2)}) collective-permute-start(bf16[1,256,512]{2,1,0:T(8,128)(2,1)S(1)} %get-tuple-element.42), channel_id=1, source_target_pairs={{0,4},{4,0},{8,12},{12,8},{1,5},{5,1},{9,13},{13,9},{2,6},{6,2},{1... | collective-permute-start | bytes 786440 | tf_op jit(solution)/shard_map/ppermute | solution.py:25
  43.0 16.2 %collective-permute-start.19 = (bf16[1,256,512]{2,1,0:T(8,128)(2,1)S(1)}, bf16[1,256,512]{2,1,0:T(8,128)(2,1)S(1)}, u32[]{:S(2)}, u32[]{:S(2)}) collective-permute-start(bf16[1,256,512]{2,1,0:T(8,128)(2,1)S(1)} %get-tuple-element.40), channel_id=1, source_target_pairs={{0,4},{4,0},{8,12},{12,8},{1,5},{5,1},{9,13},{13,9},{2,6},{6,2},{1... | collective-permute-start | bytes 786440 | tf_op jit(solution)/shard_map/ppermute | solution.py:25
  58.7 21.1 %collective-permute-start.22 = (bf16[1,256,512]{2,1,0:T(8,128)(2,1)S(1)}, bf16[1,256,512]{2,1,0:T(8,128)(2,1)S(1)}, u32[]{:S(2)}, u32[]{:S(2)}) collective-permute-start(bf16[1,256,512]{2,1,0:T(8,128)(2,1)S(1)} %collective-permute-done.21.refs_10_), channel_id=1, source_target_pairs={{0,16},{16,0},{1,17},{17,1},{2,18},{18,2},{3,19},{19,3},{4,20},{20... | collective-permute-start | bytes 786440 | tf_op jit(solution)/shard_map/ppermute | solution.py:25
  62.4 27.3 %collective-permute-start.20 = (bf16[1,256,512]{2,1,0:T(8,128)(2,1)S(1)}, bf16[1,256,512]{2,1,0:T(8,128)(2,1)S(1)}, u32[]{:S(2)}, u32[]{:S(2)}) collective-permute-start(bf16[1,256,512]{2,1,0:T(8,128)(2,1)S(1)} %collective-permute-done.19.refs_8_), channel_id=1, source_target_pairs={{0,16},{16,0},{1,17},{17,1},{2,18},{18,2},{3,19},{19,3},{4,20},{20... | collective-permute-start | bytes 786440 | tf_op jit(solution)/shard_map/ppermute | solution.py:25
  64.0 20.8 %collective-permute-start.15 = (bf16[1,256,512]{2,1,0:T(8,128)(2,1)S(1)}, bf16[1,256,512]{2,1,0:T(8,128)(2,1)S(1)}, u32[]{:S(2)}, u32[]{:S(2)}) collective-permute-start(bf16[1,256,512]{2,1,0:T(8,128)(2,1)S(1)} %collective-permute-done.14.refs_6_), channel_id=1, source_target_pairs={{0,16},{16,0},{1,17},{17,1},{2,18},{18,2},{3,19},{19,3},{4,20},{20... | collective-permute-start | bytes 786440 | tf_op jit(solution)/shard_map/ppermute | solution.py:25
  65.8 23.9 %collective-permute-start.24 = (bf16[1,256,512]{2,1,0:T(8,128)(2,1)S(1)}, bf16[1,256,512]{2,1,0:T(8,128)(2,1)S(1)}, u32[]{:S(2)}, u32[]{:S(2)}) collective-permute-start(bf16[1,256,512]{2,1,0:T(8,128)(2,1)S(1)} %collective-permute-done.23.refs_12_), channel_id=1, source_target_pairs={{0,16},{16,0},{1,17},{17,1},{2,18},{18,2},{3,19},{19,3},{4,20},{20... | collective-permute-start | bytes 786440 | tf_op jit(solution)/shard_map/ppermute | solution.py:25
  73.5 16.2 %collective-permute-start.16 = (f32[2,512]{1,0:T(2,128)S(1)}, f32[2,512]{1,0:T(2,128)S(1)}, u32[]{:S(2)}, u32[]{:S(2)}) collective-permute-start(f32[2,512]{1,0:T(2,128)S(1)} %get-tuple-element.26), channel_id=1, source_target_pairs={{0,12},{1,13},{2,14},{3,15},{16,28},{17,29},{18,30},{19,31}} | collective-permute-start | bytes 12296 | tf_op jit(solution)/shard_map/ppermute | solution.py:30
  95.4 16.9 %collective-permute-start.32 = (bf16[1,256,512]{2,1,0:T(8,128)(2,1)S(1)}, bf16[1,256,512]{2,1,0:T(8,128)(2,1)S(1)}, u32[]{:S(2)}, u32[]{:S(2)}) collective-permute-start(bf16[1,256,512]{2,1,0:T(8,128)(2,1)S(1)} %get-tuple-element.43), channel_id=1, source_target_pairs={{0,8},{4,12},{8,0},{12,4},{1,9},{5,13},{9,1},{13,5},{2,10},{6,14},... | collective-permute-start | bytes 786440 | tf_op jit(solution)/shard_map/ppermute | solution.py:25
  105.2 17.3 %collective-permute-start.28 = (bf16[384,512]{1,0:T(8,128)(2,1)S(1)}, bf16[384,512]{1,0:T(8,128)(2,1)S(1)}, u32[]{:S(2)}, u32[]{:S(2)}) collective-permute-start(bf16[384,512]{1,0:T(8,128)(2,1)S(1)} %fusion.8.refs_0_), channel_id=1, source_target_pairs={{0,2},{1,3},{2,0},{3,1},{4,6},{5,7},{6,4},{7,5},{8,10},{9,11},{10,... | collective-permute-start | bytes 1179656 | tf_op jit(solution)/shard_map/ppermute | solution.py:25
  109.1 21.5 %collective-permute-start.38 = (bf16[1,256,512]{2,1,0:T(8,128)(2,1)S(1)}, bf16[1,256,512]{2,1,0:T(8,128)(2,1)S(1)}, u32[]{:S(2)}, u32[]{:S(2)}) collective-permute-start(bf16[1,256,512]{2,1,0:T(8,128)(2,1)S(1)} %get-tuple-element.41), channel_id=1, source_target_pairs={{0,8},{4,12},{8,0},{12,4},{1,9},{5,13},{9,1},{13,5},{2,10},{6,14},... | collective-permute-start | bytes 786440 | tf_op jit(solution)/shard_map/ppermute | solution.py:25
  112.2 22.1 %collective-permute-start.48 = (bf16[1,256,512]{2,1,0:T(8,128)(2,1)S(1)}, bf16[1,256,512]{2,1,0:T(8,128)(2,1)S(1)}, u32[]{:S(2)}, u32[]{:S(2)}) collective-permute-start(bf16[1,256,512]{2,1,0:T(8,128)(2,1)S(1)} %get-tuple-element.39), channel_id=1, source_target_pairs={{0,8},{4,12},{8,0},{12,4},{1,9},{5,13},{9,1},{13,5},{2,10},{6,14},... | collective-permute-start | bytes 786440 | tf_op jit(solution)/shard_map/ppermute | solution.py:25
  112.2 23.6 %collective-permute-start.34 = (bf16[1,256,512]{2,1,0:T(8,128)(2,1)S(1)}, bf16[1,256,512]{2,1,0:T(8,128)(2,1)S(1)}, u32[]{:S(2)}, u32[]{:S(2)}) collective-permute-start(bf16[1,256,512]{2,1,0:T(8,128)(2,1)S(1)} %collective-permute-done.32.refs_8_), channel_id=1, source_target_pairs={{0,4},{4,0},{8,12},{12,8},{1,5},{5,1},{9,13},{13,9},{2,6},{6,2},{1... | collective-permute-start | bytes 786440 | tf_op jit(solution)/shard_map/ppermute | solution.py:25
  122.5 25.7 %collective-permute-start.27 = (bf16[384,512]{1,0:T(8,128)(2,1)S(1)}, bf16[384,512]{1,0:T(8,128)(2,1)S(1)}, u32[]{:S(2)}, u32[]{:S(2)}) collective-permute-start(bf16[384,512]{1,0:T(8,128)(2,1)S(1)} %fusion.8.refs_0_), channel_id=1, source_target_pairs={{0,1},{1,0},{2,3},{3,2},{4,5},{5,4},{6,7},{7,6},{8,9},{9,8},{10,11... | collective-permute-start | bytes 1179656 | tf_op jit(solution)/shard_map/ppermute | solution.py:25
  122.5 27.2 %collective-permute-start.29 = (bf16[384,512]{1,0:T(8,128)(2,1)S(1)}, bf16[384,512]{1,0:T(8,128)(2,1)S(1)}, u32[]{:S(2)}, u32[]{:S(2)}) collective-permute-start(bf16[384,512]{1,0:T(8,128)(2,1)S(1)} %collective-permute-done.28.refs_2_), channel_id=1, source_target_pairs={{0,1},{1,0},{2,3},{3,2},{4,5},{5,4},{6,7},{7,6},{8,9},{9,8},{10,11... | collective-permute-start | bytes 1179656 | tf_op jit(solution)/shard_map/ppermute | solution.py:25
  156.6 18.2 %collective-permute-start.50 = (bf16[1,256,512]{2,1,0:T(8,128)(2,1)S(1)}, bf16[1,256,512]{2,1,0:T(8,128)(2,1)S(1)}, u32[]{:S(2)}, u32[]{:S(2)}) collective-permute-start(bf16[1,256,512]{2,1,0:T(8,128)(2,1)S(1)} %collective-permute-done.48.refs_10_), channel_id=1, source_target_pairs={{0,4},{4,0},{8,12},{12,8},{1,5},{5,1},{9,13},{13,9},{2,6},{6,2},{1... | collective-permute-start | bytes 786440 | tf_op jit(solution)/shard_map/ppermute | solution.py:25
  159.5 22.9 %collective-permute-start.47 = (bf16[1,256,512]{2,1,0:T(8,128)(2,1)S(1)}, bf16[1,256,512]{2,1,0:T(8,128)(2,1)S(1)}, u32[]{:S(2)}, u32[]{:S(2)}) collective-permute-start(bf16[1,256,512]{2,1,0:T(8,128)(2,1)S(1)} %collective-permute-done.46.refs_8_), channel_id=1, source_target_pairs={{0,16},{16,0},{1,17},{17,1},{2,18},{18,2},{3,19},{19,3},{4,20},{20... | collective-permute-start | bytes 786440 | tf_op jit(solution)/shard_map/ppermute | solution.py:25
  164.2 18.1 %collective-permute-start.51 = (bf16[1,256,512]{2,1,0:T(8,128)(2,1)S(1)}, bf16[1,256,512]{2,1,0:T(8,128)(2,1)S(1)}, u32[]{:S(2)}, u32[]{:S(2)}) collective-permute-start(bf16[1,256,512]{2,1,0:T(8,128)(2,1)S(1)} %collective-permute-done.49.refs_11_), channel_id=1, source_target_pairs={{0,4},{4,0},{8,12},{12,8},{1,5},{5,1},{9,13},{13,9},{2,6},{6,2},{1... | collective-permute-start | bytes 786440 | tf_op jit(solution)/shard_map/ppermute | solution.py:25
  (45 other events, 625.6 us)
where the time goes:
time: 203 us
  waiting for transfers between devices  93.7 us (46%)
  starting transfers between devices  84.8 us (42%)
  Pallas kernels  18.4 us (9%)
  local copies, waits for them, and re-layouts  3.4 us (2%)
    ppermute x49, waiting for transfers between devices, swap(): return lax.ppermute(value, axis, [(i, i ^ mask) for i in range(count)])  89.8 us
    ppermute x49, starting transfers between devices, swap(): return lax.ppermute(value, axis, [(i, i ^ mask) for i in range(count)])  58.5 us
    ppermute x8, starting transfers between devices, shift(): lax.ppermute(value, axis, [(i, i + steps) for i in range(count - steps)])  26.3 us
    pallas_call x2, Pallas kernels, on_device(): pl.pallas_call(functools.partial(scan_kernel, pre), out_shape=(shape((cha...  8.09 us
    pallas_call x2, Pallas kernels, on_device(): pl.pallas_call(functools.partial(recur_kernel, layer, places[f'm{layer}']...  4.66 us
  transfers between devices with their start and end apart: 57, of which 23 were waited for; matrix products, arithmetic and copies ran while one was open for 1% of the time, Pallas kernels for 8%

commit v1 on v0

--- a/solution.py
+++ b/solution.py
@@ -57,9 +57,12 @@
     return parts
 
 
-def gather_tp(own):
+def gather_tp(own, far=None):
     held = {0: own}
     bit = lax.axis_size("tp") // 2
+    if far is not None:
+        held[bit] = far
+        bit //= 2
     while bit:
         for offset, value in list(held.items()):
             held[offset | bit] = swap(value, "tp", bit)
@@ -186,7 +189,7 @@
             hcum[b, at, :] = driven[:, lanes]
         return 0
 
-    lax.fori_loop(0, rows // step, one, 0, unroll=2)
+    lax.fori_loop(0, rows // step, one, 0, unroll=4)
     length = rows // SUBLANES
 
     def scan(i, carry):
@@ -206,7 +209,7 @@
     nl = channels // LANES
     ones = tuple(jnp.ones((SUBLANES, LANES), F32) for _ in range(nl))
     zeros = tuple(jnp.zeros((SUBLANES, LANES), F32) for _ in range(nl))
-    a_all, h_all = lax.fori_loop(0, length, scan, (ones, zeros), unroll=4)
+    a_all, h_all = lax.fori_loop(0, length, scan, (ones, zeros), unroll=8)
     for b in range(nl):
         lanes = slice(b * LANES, (b + 1) * LANES)
         ca, ch = jnp.ones((1, LANES), F32), jnp.zeros((1, LANES), F32)
@@ -291,11 +294,11 @@
                 chunks[f"{kind}{layer}"] = [named[kind]] + parts
                 places[f"{kind}{layer}"] = place
 
-    own = starting_stream
+    own, far = starting_stream, None
     for layer in range(layers):
         pre = HALO if layer == 0 else 0
         lead = [shift(own[rows - HALO :], "sp", 1)] if pre else []
-        pieces = gather_tp(jnp.concatenate(lead + [own], axis=0))
+        pieces = gather_tp(jnp.concatenate(lead + [own], axis=0), far)
         ws = chunks[f"m{layer}"]
         normed, recurrent = pl.pallas_call(
             functools.partial(recur_kernel, layer, places[f"m{layer}"], m, len(ws)),
@@ -383,13 +386,20 @@
             name="exit",
         )(gelu, acum, hcum, seg, *before, *ws)
         bit = 1
-        while True:
+        while bit < m // 2:
             arrived = swap(send, "tp", bit)
             total = keep.astype(F32) + arrived.astype(F32)
+            send, keep = total[1::2].astype(BF16), total[0::2]
             bit *= 2
-            if bit == m:
-                break
-            send, keep = total[1::2].astype(BF16), total[0::2]
+        if layer + 1 < layers:
+            both = jnp.concatenate([keep.astype(BF16), send], axis=0)
+            arrived = swap(both, "tp", bit)
+            total = both.astype(F32) + arrived[::-1].astype(F32)
+            old = pieces[bit][pre:].astype(F32)
+            far = (old + total[1]).astype(BF16)
+        else:
+            arrived = swap(send, "tp", bit)
+            total = keep.astype(F32) + arrived.astype(F32)
         own = (own.astype(F32) + total[0]).astype(BF16)
     floats = own.astype(F32)
     squares = jnp.sum(floats * floats, axis=1)

time: 203 us -> 203 us (level)
  starting transfers between devices: 84.8 us -> 82.5 us
    ppermute x49 -> x48, waiting for transfers between devices: 89.8 us -> 91.7 us  [swap(): return lax.ppermute(value, axis, [(i, i ^ mask) for i in range(count)])]
    ppermute x49 -> x48, starting transfers between devices: 58.5 us -> 57.2 us  [swap(): return lax.ppermute(value, axis, [(i, i ^ mask) for i in range(count)])]
  transfers between devices with their start and end apart: 57 -> 56, of which waited for: 23 -> 23; matrix products, arithmetic and copies ran while one was open for 1% -> 1% of each run, Pallas kernels for 8% -> 7%
where the time goes in v1:
time: 203 us; the launch traced here: 202 us
  waiting for transfers between devices  95.6 us (47%)
  starting transfers between devices  82.5 us (41%)
  Pallas kernels  17.6 us (9%)
  local copies, waits for them, and re-layouts  3.37 us (2%)
  other arithmetic  2.15 us (1%)
    ppermute x48, waiting for transfers between devices, swap(): return lax.ppermute(value, axis, [(i, i ^ mask) for i in range(count)])  91.7 us
    ppermute x48, starting transfers between devices, swap(): return lax.ppermute(value, axis, [(i, i ^ mask) for i in range(count)])  57.2 us
    ppermute x8, starting transfers between devices, shift(): lax.ppermute(value, axis, [(i, i + steps) for i in range(count - steps)])  25.4 us
    pallas_call x2, Pallas kernels, on_device(): pl.pallas_call(functools.partial(scan_kernel, pre), out_shape=(shape((cha...  7.23 us
    pallas_call x2, Pallas kernels, on_device(): pl.pallas_call(functools.partial(recur_kernel, layer, places[f'm{layer}']...  4.66 us
  transfers between devices with their start and end apart: 56, of which 23 were waited for; matrix products, arithmetic and copies ran while one was open for 1% of the time, Pallas kernels for 7%

profile of v1, /device:TPU:0, one launch (start us, length us, event | category | flops | bytes accessed | tf_op | source)
XLA Modules:
  0.0 201.9 jit_solution(15159094873960381075)
XLA Ops:
  1.2 4.1 %collective-permute-start.6 = (bf16[1,256,512]{2,1,0:T(8,128)(2,1)S(1)}, bf16[1,256,512]{2,1,0:T(8,128)(2,1)S(1)}, u32[]{:S(2)}, u32[]{:S(2)}) collective-permute-start(bf16[1,256,512]{2,1,0:T(8,128)(2,1)S(1)} %get-tuple-element.46), channel_id=1, source_target_pairs={{0,8},{4,12},{8,0},{12,4},{1,9},{5,13},{9,1},{13,5},{2,10},{6,14},... | collective-permute-start | bytes 786440 | tf_op jit(solution)/shard_map/ppermute | solution.py:25
  11.3 2.9 %collective-permute-start.21 = (bf16[1,256,512]{2,1,0:T(8,128)(2,1)S(1)}, bf16[1,256,512]{2,1,0:T(8,128)(2,1)S(1)}, u32[]{:S(2)}, u32[]{:S(2)}) collective-permute-start(bf16[1,256,512]{2,1,0:T(8,128)(2,1)S(1)} %get-tuple-element.42), channel_id=1, source_target_pairs={{0,8},{4,12},{8,0},{12,4},{1,9},{5,13},{9,1},{13,5},{2,10},{6,14},... | collective-permute-start | bytes 786440 | tf_op jit(solution)/shard_map/ppermute | solution.py:25
  14.2 3.9 %collective-permute-done = bf16[16,512]{1,0:T(8,128)(2,1)S(1)} collective-permute-done((bf16[16,512]{1,0:T(8,128)(2,1)S(1)}, bf16[16,512]{1,0:T(8,128)(2,1)S(1)}, u32[]{:S(2)}, u32[]{:S(2)}) %collective-permute-start) | collective-permute-done | bytes 16416 | tf_op jit(solution)/shard_map/ppermute | solution.py:30
  22.4 5.0 %collective-permute-done.2.refs_2_ = bf16[400,512]{1,0:T(8,128)(2,1)S(1)} collective-permute-done((bf16[400,512]{1,0:T(8,128)(2,1)S(1)}, bf16[400,512]{1,0:T(8,128)(2,1)S(1)}, u32[]{:S(2)}, u32[]{:S(2)}) %collective-permute-start.2) | collective-permute-done | bytes 409632 | tf_op jit(solution)/shard_map/ppermute | solution.py:25
  27.4 7.6 %collective-permute-done.12.refs_4_ = bf16[1,256,512]{2,1,0:T(8,128)(2,1)S(1)} collective-permute-done((bf16[1,256,512]{2,1,0:T(8,128)(2,1)S(1)}, bf16[1,256,512]{2,1,0:T(8,128)(2,1)S(1)}, u32[]{:S(2)}, u32[]{:S(2)}) %collective-permute-start.12) | collective-permute-done | bytes 262176 | tf_op jit(solution)/shard_map/ppermute | solution.py:25
  36.9 2.9 %collective-permute-done.21.refs_10_ = bf16[1,256,512]{2,1,0:T(8,128)(2,1)S(1)} collective-permute-done((bf16[1,256,512]{2,1,0:T(8,128)(2,1)S(1)}, bf16[1,256,512]{2,1,0:T(8,128)(2,1)S(1)}, u32[]{:S(2)}, u32[]{:S(2)}) %collective-permute-start.21) | collective-permute-done | bytes 262176 | tf_op jit(solution)/shard_map/ppermute | solution.py:25
  44.0 4.9 %collective-permute-done.5.refs_7_ = bf16[1,256,512]{2,1,0:T(8,128)(2,1)S(1)} collective-permute-done((bf16[1,256,512]{2,1,0:T(8,128)(2,1)S(1)}, bf16[1,256,512]{2,1,0:T(8,128)(2,1)S(1)}, u32[]{:S(2)}, u32[]{:S(2)}) %collective-permute-start.5) | collective-permute-done | bytes 262176 | tf_op jit(solution)/shard_map/ppermute | solution.py:25
  50.0 2.9 %collective-permute-done.9.refs_11_ = bf16[1,256,512]{2,1,0:T(8,128)(2,1)S(1)} collective-permute-done((bf16[1,256,512]{2,1,0:T(8,128)(2,1)S(1)}, bf16[1,256,512]{2,1,0:T(8,128)(2,1)S(1)}, u32[]{:S(2)}, u32[]{:S(2)}) %collective-permute-start.9) | collective-permute-done | bytes 262176 | tf_op jit(solution)/shard_map/ppermute | solution.py:25
  67.4 3.6 %scan.2 = (f32[4,384,128]{2,1,0:T(8,128)S(1)}, f32[4,384,128]{2,1,0:T(8,128)S(1)}, f32[16,512]{1,0:T(8,128)S(1)}, f32[2,512]{1,0:T(2,128)S(1)}) custom-call(bf16[400,512]{1,0:T(8,128)(2,1)S(1)} %get-tuple-element.22.refs_0_, bf16[4,512]{1,0:T(4,128)(2,1)S(1)} %get-tuple-element.54.refs_1_, bf16[2,256,256]{2,1,0:T(8,128)(2,1)S(1)} %get-tuple-element.57.refs_2_, ...), custom_call_target="tpu_custom_call" | custom-call | flops 3221225472 | bytes 6291456 | tf_op jit(solution)/shard_map/scan/pallas_call | solution.py:338
  71.0 2.6 %collective-permute-done.11.refs_3_ = bf16[1,256,512]{2,1,0:T(8,128)(2,1)S(1)} collective-permute-done((bf16[1,256,512]{2,1,0:T(8,128)(2,1)S(1)}, bf16[1,256,512]{2,1,0:T(8,128)(2,1)S(1)}, u32[]{:S(2)}, u32[]{:S(2)}) %collective-permute-start.11) | collective-permute-done | bytes 262176 | tf_op jit(solution)/shard_map/ppermute | solution.py:25
  73.5 6.3 %collective-permute-start.16 = (f32[2,512]{1,0:T(2,128)S(1)}, f32[2,512]{1,0:T(2,128)S(1)}, u32[]{:S(2)}, u32[]{:S(2)}) collective-permute-start(f32[2,512]{1,0:T(2,128)S(1)} %get-tuple-element.26), channel_id=1, source_target_pairs={{0,12},{1,13},{2,14},{3,15},{16,28},{17,29},{18,30},{19,31}} | collective-permute-start | bytes 12296 | tf_op jit(solution)/shard_map/ppermute | solution.py:30
  81.1 3.7 %collective-permute-done.15.refs_7_ = bf16[1,256,512]{2,1,0:T(8,128)(2,1)S(1)} collective-permute-done((bf16[1,256,512]{2,1,0:T(8,128)(2,1)S(1)}, bf16[1,256,512]{2,1,0:T(8,128)(2,1)S(1)}, u32[]{:S(2)}, u32[]{:S(2)}) %collective-permute-start.15) | collective-permute-done | bytes 262176 | tf_op jit(solution)/shard_map/ppermute | solution.py:25
  84.8 3.5 %collective-permute-start.18 = (f32[2,512]{1,0:T(2,128)S(1)}, f32[2,512]{1,0:T(2,128)S(1)}, u32[]{:S(2)}, u32[]{:S(2)}) collective-permute-start(f32[2,512]{1,0:T(2,128)S(1)} %get-tuple-element.26), channel_id=1, source_target_pairs={{0,4},{4,8},{8,12},{1,5},{5,9},{9,13},{2,6},{6,10},{10,14},{3,7},{... | collective-permute-start | bytes 12296 | tf_op jit(solution)/shard_map/ppermute | solution.py:30
  95.3 3.9 %collective-permute-start.31 = (bf16[1,256,512]{2,1,0:T(8,128)(2,1)S(1)}, bf16[1,256,512]{2,1,0:T(8,128)(2,1)S(1)}, u32[]{:S(2)}, u32[]{:S(2)}) collective-permute-start(bf16[1,256,512]{2,1,0:T(8,128)(2,1)S(1)} %get-tuple-element.45), channel_id=1, source_target_pairs={{0,8},{4,12},{8,0},{12,4},{1,9},{5,13},{9,1},{13,5},{2,10},{6,14},... | collective-permute-start | bytes 786440 | tf_op jit(solution)/shard_map/ppermute | solution.py:25
  100.8 2.9 %collective-permute-start.47 = (bf16[1,256,512]{2,1,0:T(8,128)(2,1)S(1)}, bf16[1,256,512]{2,1,0:T(8,128)(2,1)S(1)}, u32[]{:S(2)}, u32[]{:S(2)}) collective-permute-start(bf16[1,256,512]{2,1,0:T(8,128)(2,1)S(1)} %get-tuple-element.41), channel_id=1, source_target_pairs={{0,8},{4,12},{8,0},{12,4},{1,9},{5,13},{9,1},{13,5},{2,10},{6,14},... | collective-permute-start | bytes 786440 | tf_op jit(solution)/shard_map/ppermute | solution.py:25
  103.7 9.0 %collective-permute-done.31.refs_8_ = bf16[1,256,512]{2,1,0:T(8,128)(2,1)S(1)} collective-permute-done((bf16[1,256,512]{2,1,0:T(8,128)(2,1)S(1)}, bf16[1,256,512]{2,1,0:T(8,128)(2,1)S(1)}, u32[]{:S(2)}, u32[]{:S(2)}) %collective-permute-start.31) | collective-permute-done | bytes 262176 | tf_op jit(solution)/shard_map/ppermute | solution.py:25
  114.5 14.4 %collective-permute-done.37.refs_4_ = bf16[1,256,512]{2,1,0:T(8,128)(2,1)S(1)} collective-permute-done((bf16[1,256,512]{2,1,0:T(8,128)(2,1)S(1)}, bf16[1,256,512]{2,1,0:T(8,128)(2,1)S(1)}, u32[]{:S(2)}, u32[]{:S(2)}) %collective-permute-start.37) | collective-permute-done | bytes 262176 | tf_op jit(solution)/shard_map/ppermute | solution.py:25
  129.9 3.8 %collective-permute-done.47.refs_10_ = bf16[1,256,512]{2,1,0:T(8,128)(2,1)S(1)} collective-permute-done((bf16[1,256,512]{2,1,0:T(8,128)(2,1)S(1)}, bf16[1,256,512]{2,1,0:T(8,128)(2,1)S(1)}, u32[]{:S(2)}, u32[]{:S(2)}) %collective-permute-start.47) | collective-permute-done | bytes 262176 | tf_op jit(solution)/shard_map/ppermute | solution.py:25
  137.0 5.9 %collective-permute-done.30.refs_7_ = bf16[1,256,512]{2,1,0:T(8,128)(2,1)S(1)} collective-permute-done((bf16[1,256,512]{2,1,0:T(8,128)(2,1)S(1)}, bf16[1,256,512]{2,1,0:T(8,128)(2,1)S(1)}, u32[]{:S(2)}, u32[]{:S(2)}) %collective-permute-start.30) | collective-permute-done | bytes 262176 | tf_op jit(solution)/shard_map/ppermute | solution.py:25
  143.5 3.3 %collective-permute-done.34.refs_11_ = bf16[1,256,512]{2,1,0:T(8,128)(2,1)S(1)} collective-permute-done((bf16[1,256,512]{2,1,0:T(8,128)(2,1)S(1)}, bf16[1,256,512]{2,1,0:T(8,128)(2,1)S(1)}, u32[]{:S(2)}, u32[]{:S(2)}) %collective-permute-start.34) | collective-permute-done | bytes 262176 | tf_op jit(solution)/shard_map/ppermute | solution.py:25
  155.2 3.4 %collective-permute-start.49 = (bf16[1,256,512]{2,1,0:T(8,128)(2,1)S(1)}, bf16[1,256,512]{2,1,0:T(8,128)(2,1)S(1)}, u32[]{:S(2)}, u32[]{:S(2)}) collective-permute-start(bf16[1,256,512]{2,1,0:T(8,128)(2,1)S(1)} %collective-permute-done.47.refs_10_), channel_id=1, source_target_pairs={{0,4},{4,0},{8,12},{12,8},{1,5},{5,1},{9,13},{13,9},{2,6},{6,2},{1... | collective-permute-start | bytes 786440 | tf_op jit(solution)/shard_map/ppermute | solution.py:25
  164.1 3.6 %scan.3 = (f32[4,384,128]{2,1,0:T(8,128)S(1)}, f32[4,384,128]{2,1,0:T(8,128)S(1)}, f32[16,512]{1,0:T(8,128)S(1)}, f32[2,512]{1,0:T(2,128)S(1)}) custom-call(bf16[384,512]{1,0:T(8,128)(2,1)S(1)} %get-tuple-element.30.refs_0_, bf16[16,512]{1,0:T(8,128)(2,1)S(1)} %collective-permute-done.41.refs_1_, bf16[4,512]{1,0:T(4,128)(2,1)S(1)} %get-tuple-element.53.refs_2_, ...), custom_call_target="tpu_custom_call" | custom-call | flops 3221225472 | bytes 6291456 | tf_op jit(solution)/shard_map/scan/pallas_call | solution.py:338
  168.5 5.9 %collective-permute-start.42 = (f32[2,512]{1,0:T(2,128)S(1)}, f32[2,512]{1,0:T(2,128)S(1)}, u32[]{:S(2)}, u32[]{:S(2)}) collective-permute-start(f32[2,512]{1,0:T(2,128)S(1)} %get-tuple-element.34), channel_id=1, source_target_pairs={{0,12},{1,13},{2,14},{3,15},{16,28},{17,29},{18,30},{19,31}} | collective-permute-start | bytes 12296 | tf_op jit(solution)/shard_map/ppermute | solution.py:30
  186.3 10.6 %collective-permute-done.52 = bf16[1,384,512]{2,1,0:T(8,128)(2,1)S(1)} collective-permute-done((bf16[1,384,512]{2,1,0:T(8,128)(2,1)S(1)}, bf16[1,384,512]{2,1,0:T(8,128)(2,1)S(1)}, u32[]{:S(2)}, u32[]{:S(2)}) %collective-permute-start.52) | collective-permute-done | bytes 393248 | tf_op jit(solution)/shard_map/ppermute | solution.py:25
  (141 shorter events, 80.9 us)
Async XLA Ops:
  1.2 18.5 %collective-permute-start.6 = (bf16[1,256,512]{2,1,0:T(8,128)(2,1)S(1)}, bf16[1,256,512]{2,1,0:T(8,128)(2,1)S(1)}, u32[]{:S(2)}, u32[]{:S(2)}) collective-permute-start(bf16[1,256,512]{2,1,0:T(8,128)(2,1)S(1)} %get-tuple-element.46), channel_id=1, source_target_pairs={{0,8},{4,12},{8,0},{12,4},{1,9},{5,13},{9,1},{13,5},{2,10},{6,14},... | collective-permute-start | bytes 786440 | tf_op jit(solution)/shard_map/ppermute | solution.py:25
  5.4 16.9 %collective-permute-start.4 = (bf16[1,256,512]{2,1,0:T(8,128)(2,1)S(1)}, bf16[1,256,512]{2,1,0:T(8,128)(2,1)S(1)}, u32[]{:S(2)}, u32[]{:S(2)}) collective-permute-start(bf16[1,256,512]{2,1,0:T(8,128)(2,1)S(1)} %get-tuple-element.46), channel_id=1, source_target_pairs={{0,4},{4,0},{8,12},{12,8},{1,5},{5,1},{9,13},{13,9},{2,6},{6,2},{1... | collective-permute-start | bytes 786440 | tf_op jit(solution)/shard_map/ppermute | solution.py:25
  11.1 24.0 %collective-permute-start.12 = (bf16[1,256,512]{2,1,0:T(8,128)(2,1)S(1)}, bf16[1,256,512]{2,1,0:T(8,128)(2,1)S(1)}, u32[]{:S(2)}, u32[]{:S(2)}) collective-permute-start(bf16[1,256,512]{2,1,0:T(8,128)(2,1)S(1)} %get-tuple-element.44), channel_id=1, source_target_pairs={{0,8},{4,12},{8,0},{12,4},{1,9},{5,13},{9,1},{13,5},{2,10},{6,14},... | collective-permute-start | bytes 786440 | tf_op jit(solution)/shard_map/ppermute | solution.py:25
  11.3 28.5 %collective-permute-start.21 = (bf16[1,256,512]{2,1,0:T(8,128)(2,1)S(1)}, bf16[1,256,512]{2,1,0:T(8,128)(2,1)S(1)}, u32[]{:S(2)}, u32[]{:S(2)}) collective-permute-start(bf16[1,256,512]{2,1,0:T(8,128)(2,1)S(1)} %get-tuple-element.42), channel_id=1, source_target_pairs={{0,8},{4,12},{8,0},{12,4},{1,9},{5,13},{9,1},{13,5},{2,10},{6,14},... | collective-permute-start | bytes 786440 | tf_op jit(solution)/shard_map/ppermute | solution.py:25
  19.7 21.7 %collective-permute-start.8 = (bf16[1,256,512]{2,1,0:T(8,128)(2,1)S(1)}, bf16[1,256,512]{2,1,0:T(8,128)(2,1)S(1)}, u32[]{:S(2)}, u32[]{:S(2)}) collective-permute-start(bf16[1,256,512]{2,1,0:T(8,128)(2,1)S(1)} %collective-permute-done.6.refs_8_), channel_id=1, source_target_pairs={{0,4},{4,0},{8,12},{12,8},{1,5},{5,1},{9,13},{13,9},{2,6},{6,2},{1... | collective-permute-start | bytes 786440 | tf_op jit(solution)/shard_map/ppermute | solution.py:25
  22.3 19.7 %collective-permute-start.1 = (bf16[400,512]{1,0:T(8,128)(2,1)S(1)}, bf16[400,512]{1,0:T(8,128)(2,1)S(1)}, u32[]{:S(2)}, u32[]{:S(2)}) collective-permute-start(bf16[400,512]{1,0:T(8,128)(2,1)S(1)} %constant_dynamic-update-slice_fusion.refs_0_), channel_id=1, source_target_pairs={{0,1},{1,0},{2,3},{3,2},{4,5},{5,4},{6,7},{7,6},{8,9},{9,8},{10,11... | collective-permute-start | bytes 1228808 | tf_op jit(solution)/shard_map/ppermute | solution.py:25
  27.4 27.1 %collective-permute-start.3 = (bf16[400,512]{1,0:T(8,128)(2,1)S(1)}, bf16[400,512]{1,0:T(8,128)(2,1)S(1)}, u32[]{:S(2)}, u32[]{:S(2)}) collective-permute-start(bf16[400,512]{1,0:T(8,128)(2,1)S(1)} %collective-permute-done.2.refs_2_), channel_id=1, source_target_pairs={{0,1},{1,0},{2,3},{3,2},{4,5},{5,4},{6,7},{7,6},{8,9},{9,8},{10,11... | collective-permute-start | bytes 1228808 | tf_op jit(solution)/shard_map/ppermute | solution.py:25
  42.0 16.7 %collective-permute-start.10 = (bf16[1,256,512]{2,1,0:T(8,128)(2,1)S(1)}, bf16[1,256,512]{2,1,0:T(8,128)(2,1)S(1)}, u32[]{:S(2)}, u32[]{:S(2)}) collective-permute-start(bf16[1,256,512]{2,1,0:T(8,128)(2,1)S(1)} %get-tuple-element.44), channel_id=1, source_target_pairs={{0,4},{4,0},{8,12},{12,8},{1,5},{5,1},{9,13},{13,9},{2,6},{6,2},{1... | collective-permute-start | bytes 786440 | tf_op jit(solution)/shard_map/ppermute | solution.py:25
  43.0 16.2 %collective-permute-start.19 = (bf16[1,256,512]{2,1,0:T(8,128)(2,1)S(1)}, bf16[1,256,512]{2,1,0:T(8,128)(2,1)S(1)}, u32[]{:S(2)}, u32[]{:S(2)}) collective-permute-start(bf16[1,256,512]{2,1,0:T(8,128)(2,1)S(1)} %get-tuple-element.42), channel_id=1, source_target_pairs={{0,4},{4,0},{8,12},{12,8},{1,5},{5,1},{9,13},{13,9},{2,6},{6,2},{1... | collective-permute-start | bytes 786440 | tf_op jit(solution)/shard_map/ppermute | solution.py:25
  58.7 21.1 %collective-permute-start.22 = (bf16[1,256,512]{2,1,0:T(8,128)(2,1)S(1)}, bf16[1,256,512]{2,1,0:T(8,128)(2,1)S(1)}, u32[]{:S(2)}, u32[]{:S(2)}) collective-permute-start(bf16[1,256,512]{2,1,0:T(8,128)(2,1)S(1)} %collective-permute-done.21.refs_10_), channel_id=1, source_target_pairs={{0,16},{16,0},{1,17},{17,1},{2,18},{18,2},{3,19},{19,3},{4,20},{20... | collective-permute-start | bytes 786440 | tf_op jit(solution)/shard_map/ppermute | solution.py:25
  62.4 27.2 %collective-permute-start.20 = (bf16[1,256,512]{2,1,0:T(8,128)(2,1)S(1)}, bf16[1,256,512]{2,1,0:T(8,128)(2,1)S(1)}, u32[]{:S(2)}, u32[]{:S(2)}) collective-permute-start(bf16[1,256,512]{2,1,0:T(8,128)(2,1)S(1)} %collective-permute-done.19.refs_8_), channel_id=1, source_target_pairs={{0,16},{16,0},{1,17},{17,1},{2,18},{18,2},{3,19},{19,3},{4,20},{20... | collective-permute-start | bytes 786440 | tf_op jit(solution)/shard_map/ppermute | solution.py:25
  64.0 20.8 %collective-permute-start.15 = (bf16[1,256,512]{2,1,0:T(8,128)(2,1)S(1)}, bf16[1,256,512]{2,1,0:T(8,128)(2,1)S(1)}, u32[]{:S(2)}, u32[]{:S(2)}) collective-permute-start(bf16[1,256,512]{2,1,0:T(8,128)(2,1)S(1)} %collective-permute-done.14.refs_6_), channel_id=1, source_target_pairs={{0,16},{16,0},{1,17},{17,1},{2,18},{18,2},{3,19},{19,3},{4,20},{20... | collective-permute-start | bytes 786440 | tf_op jit(solution)/shard_map/ppermute | solution.py:25
  65.8 23.9 %collective-permute-start.24 = (bf16[1,256,512]{2,1,0:T(8,128)(2,1)S(1)}, bf16[1,256,512]{2,1,0:T(8,128)(2,1)S(1)}, u32[]{:S(2)}, u32[]{:S(2)}) collective-permute-start(bf16[1,256,512]{2,1,0:T(8,128)(2,1)S(1)} %collective-permute-done.23.refs_12_), channel_id=1, source_target_pairs={{0,16},{16,0},{1,17},{17,1},{2,18},{18,2},{3,19},{19,3},{4,20},{20... | collective-permute-start | bytes 786440 | tf_op jit(solution)/shard_map/ppermute | solution.py:25
  93.8 19.6 %collective-permute-start.26 = (bf16[2,384,512]{2,1,0:T(8,128)(2,1)S(1)}, bf16[2,384,512]{2,1,0:T(8,128)(2,1)S(1)}, u32[]{:S(2)}, u32[]{:S(2)}) collective-permute-start(bf16[2,384,512]{2,1,0:T(8,128)(2,1)S(1)} %add_convert_fusion), channel_id=1, source_target_pairs={{0,2},{1,3},{2,0},{3,1},{4,6},{5,7},{6,4},{7,5},{8,10},{9,11},{10,... | collective-permute-start | bytes 2359304 | tf_op jit(solution)/shard_map/ppermute | solution.py:25
  95.3 17.4 %collective-permute-start.31 = (bf16[1,256,512]{2,1,0:T(8,128)(2,1)S(1)}, bf16[1,256,512]{2,1,0:T(8,128)(2,1)S(1)}, u32[]{:S(2)}, u32[]{:S(2)}) collective-permute-start(bf16[1,256,512]{2,1,0:T(8,128)(2,1)S(1)} %get-tuple-element.45), channel_id=1, source_target_pairs={{0,8},{4,12},{8,0},{12,4},{1,9},{5,13},{9,1},{13,5},{2,10},{6,14},... | collective-permute-start | bytes 786440 | tf_op jit(solution)/shard_map/ppermute | solution.py:25
  100.8 28.1 %collective-permute-start.37 = (bf16[1,256,512]{2,1,0:T(8,128)(2,1)S(1)}, bf16[1,256,512]{2,1,0:T(8,128)(2,1)S(1)}, u32[]{:S(2)}, u32[]{:S(2)}) collective-permute-start(bf16[1,256,512]{2,1,0:T(8,128)(2,1)S(1)} %get-tuple-element.43), channel_id=1, source_target_pairs={{0,8},{4,12},{8,0},{12,4},{1,9},{5,13},{9,1},{13,5},{2,10},{6,14},... | collective-permute-start | bytes 786440 | tf_op jit(solution)/shard_map/ppermute | solution.py:25
  100.8 32.9 %collective-permute-start.47 = (bf16[1,256,512]{2,1,0:T(8,128)(2,1)S(1)}, bf16[1,256,512]{2,1,0:T(8,128)(2,1)S(1)}, u32[]{:S(2)}, u32[]{:S(2)}) collective-permute-start(bf16[1,256,512]{2,1,0:T(8,128)(2,1)S(1)} %get-tuple-element.41), channel_id=1, source_target_pairs={{0,8},{4,12},{8,0},{12,4},{1,9},{5,13},{9,1},{13,5},{2,10},{6,14},... | collective-permute-start | bytes 786440 | tf_op jit(solution)/shard_map/ppermute | solution.py:25
  112.7 22.0 %collective-permute-start.33 = (bf16[1,256,512]{2,1,0:T(8,128)(2,1)S(1)}, bf16[1,256,512]{2,1,0:T(8,128)(2,1)S(1)}, u32[]{:S(2)}, u32[]{:S(2)}) collective-permute-start(bf16[1,256,512]{2,1,0:T(8,128)(2,1)S(1)} %collective-permute-done.31.refs_8_), channel_id=1, source_target_pairs={{0,4},{4,0},{8,12},{12,8},{1,5},{5,1},{9,13},{13,9},{2,6},{6,2},{1... | collective-permute-start | bytes 786440 | tf_op jit(solution)/shard_map/ppermute | solution.py:25
  114.0 34.3 %collective-permute-start.27 = (bf16[384,512]{1,0:T(8,128)(2,1)S(1)}, bf16[384,512]{1,0:T(8,128)(2,1)S(1)}, u32[]{:S(2)}, u32[]{:S(2)}) collective-permute-start(bf16[384,512]{1,0:T(8,128)(2,1)S(1)} %get-tuple-element.40.refs_0_), channel_id=1, source_target_pairs={{0,1},{1,0},{2,3},{3,2},{4,5},{5,4},{6,7},{7,6},{8,9},{9,8},{10,11... | collective-permute-start | bytes 1179656 | tf_op jit(solution)/shard_map/ppermute | solution.py:25
  114.0 35.2 %collective-permute-start.28 = (bf16[384,512]{1,0:T(8,128)(2,1)S(1)}, bf16[384,512]{1,0:T(8,128)(2,1)S(1)}, u32[]{:S(2)}, u32[]{:S(2)}) collective-permute-start(bf16[384,512]{1,0:T(8,128)(2,1)S(1)} %get-tuple-element.39.refs_2_), channel_id=1, source_target_pairs={{0,1},{1,0},{2,3},{3,2},{4,5},{5,4},{6,7},{7,6},{8,9},{9,8},{10,11... | collective-permute-start | bytes 1179656 | tf_op jit(solution)/shard_map/ppermute | solution.py:25
  135.7 16.9 %collective-permute-start.35 = (bf16[1,256,512]{2,1,0:T(8,128)(2,1)S(1)}, bf16[1,256,512]{2,1,0:T(8,128)(2,1)S(1)}, u32[]{:S(2)}, u32[]{:S(2)}) collective-permute-start(bf16[1,256,512]{2,1,0:T(8,128)(2,1)S(1)} %get-tuple-element.43), channel_id=1, source_target_pairs={{0,4},{4,0},{8,12},{12,8},{1,5},{5,1},{9,13},{13,9},{2,6},{6,2},{1... | collective-permute-start | bytes 786440 | tf_op jit(solution)/shard_map/ppermute | solution.py:25
  155.2 19.3 %collective-permute-start.49 = (bf16[1,256,512]{2,1,0:T(8,128)(2,1)S(1)}, bf16[1,256,512]{2,1,0:T(8,128)(2,1)S(1)}, u32[]{:S(2)}, u32[]{:S(2)}) collective-permute-start(bf16[1,256,512]{2,1,0:T(8,128)(2,1)S(1)} %collective-permute-done.47.refs_10_), channel_id=1, source_target_pairs={{0,4},{4,0},{8,12},{12,8},{1,5},{5,1},{9,13},{13,9},{2,6},{6,2},{1... | collective-permute-start | bytes 786440 | tf_op jit(solution)/shard_map/ppermute | solution.py:25
  159.6 22.0 %collective-permute-start.46 = (bf16[1,256,512]{2,1,0:T(8,128)(2,1)S(1)}, bf16[1,256,512]{2,1,0:T(8,128)(2,1)S(1)}, u32[]{:S(2)}, u32[]{:S(2)}) collective-permute-start(bf16[1,256,512]{2,1,0:T(8,128)(2,1)S(1)} %collective-permute-done.45.refs_8_), channel_id=1, source_target_pairs={{0,16},{16,0},{1,17},{17,1},{2,18},{18,2},{3,19},{19,3},{4,20},{20... | collective-permute-start | bytes 786440 | tf_op jit(solution)/shard_map/ppermute | solution.py:25
  163.9 17.6 %collective-permute-start.50 = (bf16[1,256,512]{2,1,0:T(8,128)(2,1)S(1)}, bf16[1,256,512]{2,1,0:T(8,128)(2,1)S(1)}, u32[]{:S(2)}, u32[]{:S(2)}) collective-permute-start(bf16[1,256,512]{2,1,0:T(8,128)(2,1)S(1)} %collective-permute-done.48.refs_11_), channel_id=1, source_target_pairs={{0,4},{4,0},{8,12},{12,8},{1,5},{5,1},{9,13},{13,9},{2,6},{6,2},{1... | collective-permute-start | bytes 786440 | tf_op jit(solution)/shard_map/ppermute | solution.py:25
  (44 other events, 613.1 us)
